TPU v7x, 32 devices: a whole 2x2x4 slice. The times are simulated.
32 devices in a mesh: sp: 8 (over z, y), tp: 4 (over x, core).
Axes of the slice: x: 2, y: 2, z: 4, core: 2. Of those that a mesh axis runs over, the one named last changes fastest.
Arguments:
- stream: bfloat16 [3072, 2048], P(('sp', 'tp')), may hold values from -6 to 6
- query_projected: bfloat16 [3072, 1024], P('sp', 'tp'), may hold values from -6 to 6
- key_projected: bfloat16 [3072, 1024], P('sp', 'tp'), may hold values from -6 to 6
- value_projected: bfloat16 [3072, 1024], P('sp', 'tp'), may hold values from -6 to 6
- gate_projected: bfloat16 [3072, 1024], P('sp', 'tp'), may hold values from -6 to 6
- strength_logits: bfloat16 [8, 3072], P('tp', 'sp'), may hold values from -7 to 4
- decay_preactivation: bfloat16 [8, 3072], P('tp', 'sp'), may hold values from -9 to 9
- extra_log_decay: float32 [8, 3072], P('tp', 'sp'), may hold values from -0.7 to 0
- head_decay_rate: float32 [8], P('tp'), may hold values from 0 to 0.1
- head_norm_gain: float32 [128], replicated, may hold values from 0.1 to 1.9
- head_output_matrix: bfloat16 [1024, 2048], P('tp'), may hold values from -0.1875 to 0.1875
- feed_norm_gain: float32 [2048], replicated, may hold values from 0.1 to 1.9
- gate_matrix: bfloat16 [2048, 5632], P('sp', 'tp'), may hold values from -0.125 to 0.125
- up_matrix: bfloat16 [2048, 5632], P('sp', 'tp'), may hold values from -0.125 to 0.125
- down_matrix: bfloat16 [5632, 2048], P('tp', 'sp'), may hold values from -0.078125 to 0.078125
Outputs:
- result: bfloat16 [3072, 2048], P(('sp', 'tp'))
All inputs are finite; a program needn't handle non-finite values.
Results may differ from a plain program's by a relative error of at most 0.015.
Values may be sent and summed in bfloat16 or wider, within the bound.
No kernel may reach another device: no remote copies, remote signals or barrier semaphores. Data moves between devices by JAX's collectives and lax.ppermute only.
A program may use at most 128 MiB of HBM per device.

v0:
```python
import jax
import jax.numpy as jnp
from jax import lax
from jax.sharding import PartitionSpec as P

HEAD = 128
BLOCK = 64
PRECISION_FULL = lax.Precision.HIGHEST
EPSILON = 1e-06


def from_behind(value, axis, by):
    size = lax.axis_size(axis)
    pairs = [(i, i + by) for i in range(size) if 0 <= i + by < size]
    return lax.ppermute(value, axis, pairs)


def unit_rows(tensor):
    return tensor * lax.rsqrt(jnp.sum(tensor * tensor, axis=-1, keepdims=True) + EPSILON)


def rms_scale(tensor):
    return tensor * lax.rsqrt(jnp.mean(tensor * tensor, axis=-1, keepdims=True) + EPSILON)


def unit_lower_inverse(strict_lower):
    size = strict_lower.shape[-1]
    row = jnp.arange(size)[:, None]
    column = jnp.arange(size)[None, :]

    def corner(half):
        same_pair = row // (2 * half) == column // (2 * half)
        return jnp.where(same_pair & (row // half != column // half), strict_lower, 0.0)

    inverse = jnp.eye(size, dtype=jnp.float32) - corner(1)
    half = 2
    while half < size:
        left = jnp.einsum("hnij,hnjk->hnik", inverse, corner(half), precision=PRECISION_FULL)
        inverse = inverse - jnp.einsum("hnij,hnjk->hnik", left, inverse, precision=PRECISION_FULL)
        half *= 2
    return inverse


def swap(value, axis, bit):
    size = lax.axis_size(axis)
    return lax.ppermute(value, axis, [(i, i ^ bit) for i in range(size)])


def relative_order(count):
    order = [0]
    bit = count // 2
    while bit:
        order = order + [place ^ bit for place in order]
        bit //= 2
    return order


def gather_relative(own):
    bit = lax.axis_size("tp") // 2
    while bit:
        own = jnp.concatenate([own, swap(own, "tp", bit)], axis=0)
        bit //= 2
    return own


def scatter_relative(left_rows, matrix):
    size = lax.axis_size("tp")
    if size == 1:
        return jnp.dot(left_rows, matrix, preferred_element_type=jnp.float32)
    half = left_rows.shape[0] // 2
    leaving = jnp.dot(left_rows[half:], matrix, preferred_element_type=jnp.float32)
    arrived = swap(leaving.astype(jnp.bfloat16), "tp", 1)
    total = jnp.dot(left_rows[:half], matrix, preferred_element_type=jnp.float32)
    total = total + arrived.astype(jnp.float32)
    bit = 2
    while bit < size:
        half = total.shape[0] // 2
        arrived = swap(total[half:].astype(jnp.bfloat16), "tp", bit)
        total = total[:half] + arrived.astype(jnp.float32)
        bit *= 2
    return total


def inflow_of_earlier(matrix_product, running_state):
    size = lax.axis_size("sp")
    width = running_state.shape[-1]
    pair = jnp.concatenate([matrix_product, running_state], axis=-1)
    pair = from_behind(pair.astype(jnp.bfloat16), "sp", 1).astype(jnp.float32)
    by = 1
    while by < size - 1:
        matrix, state = (pair[..., :width], pair[..., width:])
        last = 2 * by >= size - 1
        sent = (state if last else pair).astype(jnp.bfloat16)
        earlier = from_behind(sent, "sp", by).astype(jnp.float32)
        moved = jnp.einsum("hij,hjk->hik", matrix, earlier, precision=PRECISION_FULL)
        if last:
            pair = jnp.concatenate([matrix, state + moved], axis=-1)
        else:
            pair = jnp.concatenate([moved[..., :width], state + moved[..., width:]], axis=-1)
        by *= 2
    return pair[..., width:]


def block_correction(
    unit_queries,
    unit_keys,
    complete_values,
    strength_logits,
    decay_preactivation,
    extra_log_decay,
    head_decay_rate,
):
    head_count, length, head_width = unit_queries.shape
    block_count = length // BLOCK

    def to_blocks(tensor):
        return tensor.reshape((head_count, block_count, BLOCK) + tensor.shape[2:])

    beta_gate = jax.nn.sigmoid(strength_logits.astype(jnp.float32))
    decay_logarithm = (
        -head_decay_rate[:, None] * jax.nn.softplus(decay_preactivation.astype(jnp.float32))
        + extra_log_decay
    )
    query_block = to_blocks(unit_queries)
    key_block = to_blocks(unit_keys)
    value_block = to_blocks(complete_values)
    beta_block = to_blocks(beta_gate)
    cumulative = jnp.cumsum(to_blocks(decay_logarithm), axis=-1)
    causal = jnp.tril(jnp.ones((BLOCK, BLOCK), bool))
    strict = jnp.tril(jnp.ones((BLOCK, BLOCK), bool), -1)
    spread = cumulative[..., :, None] - cumulative[..., None, :]
    damping = jnp.where(causal, jnp.exp(jnp.where(causal, spread, 0.0)), 0.0)
    key_beta = key_block * beta_block[..., None]
    lower_part = jnp.einsum(
        "hnid,hnjd->hnij", key_beta, key_block, precision=PRECISION_FULL
    ) * jnp.where(strict, damping, 0.0)
    right_side = jnp.concatenate(
        [value_block * beta_block[..., None], key_beta * jnp.exp(cumulative)[..., None]], axis=-1
    )
    solved = jnp.einsum(
        "hnij,hnjd->hnid", unit_lower_inverse(lower_part), right_side, precision=PRECISION_FULL
    )
    target_values = solved[..., :head_width]
    householder_weights = solved[..., head_width:]
    inner_scores = (
        jnp.einsum("hnid,hnjd->hnij", query_block, key_block, precision=PRECISION_FULL) * damping
    )
    decayed_queries = query_block * jnp.exp(cumulative)[..., None]
    closing_log_decay = cumulative[..., -1:]
    decayed_keys = key_block * jnp.exp(closing_log_decay - cumulative)[..., None]
    return (
        decayed_queries,
        decayed_keys,
        target_values,
        householder_weights,
        inner_scores,
        closing_log_decay,
    )


def local_recurrence(
    query_projected,
    key_projected,
    value_projected,
    strength_logits,
    decay_preactivation,
    extra_log_decay,
    head_decay_rate,
):
    head_count = strength_logits.shape[0]
    tok_count = strength_logits.shape[1]

    def split_heads(tensor):
        return tensor.reshape(tok_count, head_count, HEAD).transpose(1, 0, 2).astype(jnp.float32)

    unit_queries = unit_rows(split_heads(query_projected)) * HEAD ** (-0.5)
    unit_keys = unit_rows(split_heads(key_projected))
    complete_values = split_heads(value_projected)
    score_terms = block_correction(
        unit_queries,
        unit_keys,
        complete_values,
        strength_logits,
        decay_preactivation,
        extra_log_decay,
        head_decay_rate,
    )
    identity = jnp.broadcast_to(jnp.eye(HEAD, dtype=jnp.float32), (head_count, HEAD, HEAD))

    def advance(carry, items):
        running_state, matrix_product = carry
        (
            decayed_queries,
            decayed_keys,
            target_values,
            householder_weights,
            inner_scores,
            closing_log_decay,
        ) = items
        new_state = target_values - jnp.einsum(
            "fdc,fcj->fdj", householder_weights, running_state, precision=PRECISION_FULL
        )
        layer_output = jnp.einsum(
            "fdc,fcj->fdj", decayed_queries, running_state, precision=PRECISION_FULL
        )
        layer_output = layer_output + jnp.einsum(
            "hij,hjv->hiv", inner_scores, new_state, precision=PRECISION_FULL
        )
        passed_state = decayed_queries - jnp.einsum(
            "hij,hjk->hik", inner_scores, householder_weights, precision=PRECISION_FULL
        )
        decay_span = jnp.einsum(
            "fdc,fcj->fdj", passed_state, matrix_product, precision=PRECISION_FULL
        )
        decay_factor = jnp.exp(closing_log_decay)[:, :, None]
        step_map = decay_factor * identity - jnp.einsum(
            "hik,hij->hkj", decayed_keys, householder_weights, precision=PRECISION_FULL
        )
        running_state = decay_factor * running_state + jnp.einsum(
            "xwp,xws->xps", decayed_keys, new_state, precision=PRECISION_FULL
        )
        matrix_product = jnp.einsum(
            "hij,hjk->hik", step_map, matrix_product, precision=PRECISION_FULL
        )
        return ((running_state, matrix_product), (layer_output, decay_span))

    moved = tuple((jnp.moveaxis(tensor, 1, 0) for tensor in score_terms))
    zeros_state = jnp.zeros((head_count, HEAD, HEAD), jnp.float32)
    (running_state, matrix_product), (block_outputs, decay_spans) = lax.scan(
        advance, (zeros_state, identity), moved
    )

    def merge_blocks(tensor):
        return jnp.moveaxis(tensor, 0, 1).reshape(head_count, tok_count, HEAD)

    return (
        merge_blocks(block_outputs),
        merge_blocks(decay_spans),
        matrix_product,
        running_state,
        identity,
    )


def body(
    stream,
    query_projected,
    key_projected,
    value_projected,
    gate_projected,
    strength_logits,
    decay_preactivation,
    extra_log_decay,
    head_decay_rate,
    head_norm_gain,
    head_output_matrix,
    feed_norm_gain,
    gate_matrix,
    up_matrix,
    down_matrix,
):
    gate_whole = lax.all_gather(gate_matrix, "sp", axis=0, tiled=True)
    up_whole = lax.all_gather(up_matrix, "sp", axis=0, tiled=True)
    down_whole = lax.all_gather(down_matrix, "sp", axis=1, tiled=True)
    block_outputs, decay_spans, matrix_product, running_state, _ = local_recurrence(
        query_projected,
        key_projected,
        value_projected,
        strength_logits,
        decay_preactivation,
        extra_log_decay,
        head_decay_rate,
    )
    state_inflow = inflow_of_earlier(matrix_product, running_state)
    attention_output = block_outputs + jnp.einsum(
        "qwc,qcn->qwn", decay_spans, state_inflow, precision=PRECISION_FULL
    )
    head_count = attention_output.shape[0]
    tok_count = attention_output.shape[1]
    normed_heads = rms_scale(attention_output) * head_norm_gain
    gated = normed_heads.transpose(1, 0, 2).reshape(tok_count, head_count * HEAD)
    mixed = (gated * jax.nn.silu(gate_projected.astype(jnp.float32))).astype(jnp.bfloat16)
    tp_size = lax.axis_size("tp")
    tp_index = lax.axis_index("tp")
    chunks = mixed.reshape(tp_size, tok_count // tp_size, head_count * HEAD)
    ordered = jnp.concatenate(
        [
            lax.dynamic_index_in_dim(chunks, tp_index ^ place, 0, keepdims=False)
            for place in relative_order(tp_size)
        ],
        axis=0,
    )
    branch = scatter_relative(ordered, head_output_matrix)
    residual_own = stream.astype(jnp.float32) + branch
    normed_own = (rms_scale(residual_own) * feed_norm_gain).astype(jnp.bfloat16)
    whole_rows = gather_relative(normed_own)
    gate_total = jnp.dot(whole_rows, gate_whole, preferred_element_type=jnp.float32)
    up_total = jnp.dot(whole_rows, up_whole, preferred_element_type=jnp.float32)
    hidden = (jax.nn.silu(gate_total) * up_total).astype(jnp.bfloat16)
    ffn_own = scatter_relative(hidden, down_whole)
    return (residual_own + ffn_own).astype(jnp.bfloat16)


def solution(mesh):
    placed = (
        P(("sp", "tp"), None),
        P("sp", "tp"),
        P("sp", "tp"),
        P("sp", "tp"),
        P("sp", "tp"),
        P("tp", "sp"),
        P("tp", "sp"),
        P("tp", "sp"),
        P("tp"),
        P(),
        P("tp", None),
        P(),
        P("sp", "tp"),
        P("sp", "tp"),
        P("tp", "sp"),
    )
    return jax.shard_map(
        body, mesh=mesh, in_specs=placed, out_specs=P(("sp", "tp"), None), check_vma=False
    )
```

profile of v0, /device:TPU:0, one launch (start us, length us, event | category | flops | bytes accessed | tf_op | source)
XLA Modules:
  0.0 326.3 jit_solution(2462705551969413879)
XLA Ops:
  6.6 0.7 all-gather.4.cloned.1.call-update
  7.3 0.7 all-gather.6.cloned.1.call-update
  8.1 0.7 all-gather.8.cloned.1.call-update
  9.6 0.4 reduce_window_sum.11
  10.2 0.8 convolution_multiply_fusion
  11.2 0.5 fusion.73
  11.7 0.5 convolution_subtract_fusion.7
  12.3 0.5 fusion.71
  12.8 0.5 convolution_subtract_fusion.6
  13.3 0.5 fusion.69
  13.9 0.5 convolution_subtract_fusion.5
  14.4 0.5 fusion.67
  14.9 0.5 convolution_subtract_fusion.4
  15.5 0.5 fusion.65
  16.0 0.5 convolution_subtract_fusion.3
  17.4 0.8 fusion.42
  18.3 0.8 slice_bitcast_fusion
  19.1 0.8 fusion.38
  20.0 26.2 %while.17 = (s32[]{:T(128)}, f32[2,128,128]{2,1,0:T(8,128)S(1)}, f32[2,128,128]{2,1,0:T(8,128)S(1)}, f32[6,2,64,128]{3,2,0,1:T(8,128)}, f32[6,2,64,128]{3,2,0,1:...) while((s32[]{:T(128)}, f32[2,128,128]{2,1,0:T(8,128)S(1)}, ...), condition=%wide.region_4.5_spmd.clone, body=%wide.region_3.4_spmd.clone.sunk | while | flops 201605120 | bytes 2758829 | solution.py:229
  20.0 1.1 convolution_subtract_fusion.11
  21.4 0.8 fusion.205
  22.2 0.4 convolution_add_fusion.5
  22.8 0.9 fusion.206
  24.4 1.1 convolution_subtract_fusion.11
  25.7 0.8 fusion.205
  26.6 0.4 convolution_add_fusion.5
  27.2 0.9 fusion.206
  28.7 1.1 convolution_subtract_fusion.11
  30.1 0.8 fusion.205
  31.6 0.9 fusion.206
  33.1 1.1 convolution_subtract_fusion.11
  34.5 0.8 fusion.205
  35.3 0.4 convolution_add_fusion.5
  35.9 0.9 fusion.206
  37.5 1.1 convolution_subtract_fusion.11
  38.8 0.8 fusion.205
  40.3 0.9 fusion.206
  41.8 1.1 convolution_subtract_fusion.11
  43.2 0.8 fusion.205
  44.7 0.9 fusion.206
  46.3 5.0 %collective-permute-start = (bf16[2,128,256]{2,1,0:T(8,128)(2,1)S(1)}, bf16[2,128,256]{2,1,0:T(8,128)(2,1)S(1)}, u32[]{:S(2)}, u32[]{:S(2)}) collective-permute-start(bf16[2,128,256]{2,1,0:T(8,128)(2,1)S(1)} %pad_maximum_fusion.6), channel_id=1, source_target_pairs={{0,4},{4,8},{8,12},{12,16},{16,20},{20,24},{24,28},{1,5},{5,9},{9,... | collective-permute-start | bytes 393224 | tf_op jit(solution)/shard_map/ppermute | solution.py:15
  51.3 5.5 %collective-permute-done = bf16[2,128,256]{2,1,0:T(8,128)(2,1)S(1)} collective-permute-done((bf16[2,128,256]{2,1,0:T(8,128)(2,1)S(1)}, bf16[2,128,256]{2,1,0:T(8,128)(2,1)S(1)}, u32[]{:S(2)}, u32[]{:S(2)}) %collective-permute-start) | collective-permute-done | bytes 131104 | tf_op jit(solution)/shard_map/ppermute | solution.py:15
  56.9 4.4 %collective-permute-start.1 = (bf16[2,128,256]{2,1,0:T(8,128)(2,1)S(1)}, bf16[2,128,256]{2,1,0:T(8,128)(2,1)S(1)}, u32[]{:S(2)}, u32[]{:S(2)}) collective-permute-start(bf16[2,128,256]{2,1,0:T(8,128)(2,1)S(1)} %collective-permute-done), channel_id=1, source_target_pairs={{0,4},{4,8},{8,12},{12,16},{16,20},{20,24},{24,28},{1,5},{5,9},{9,... | collective-permute-start | bytes 393224 | tf_op jit(solution)/shard_map/ppermute | solution.py:15
  61.2 5.4 %collective-permute-done.1 = bf16[2,128,256]{2,1,0:T(8,128)(2,1)S(1)} collective-permute-done((bf16[2,128,256]{2,1,0:T(8,128)(2,1)S(1)}, bf16[2,128,256]{2,1,0:T(8,128)(2,1)S(1)}, u32[]{:S(2)}, u32[]{:S(2)}) %collective-permute-start.1) | collective-permute-done | bytes 131104 | tf_op jit(solution)/shard_map/ppermute | solution.py:15
  66.9 6.0 %collective-permute-start.2 = (bf16[2,128,256]{2,1,0:T(8,128)(2,1)S(1)}, bf16[2,128,256]{2,1,0:T(8,128)(2,1)S(1)}, u32[]{:S(2)}, u32[]{:S(2)}) collective-permute-start(bf16[2,128,256]{2,1,0:T(8,128)(2,1)S(1)} %pad_maximum_fusion.7), channel_id=1, source_target_pairs={{0,8},{4,12},{8,16},{12,20},{16,24},{20,28},{1,9},{5,13},{9,17},{1... | collective-permute-start | bytes 393224 | tf_op jit(solution)/shard_map/ppermute | solution.py:15
  72.9 5.4 %collective-permute-done.2 = bf16[2,128,256]{2,1,0:T(8,128)(2,1)S(1)} collective-permute-done((bf16[2,128,256]{2,1,0:T(8,128)(2,1)S(1)}, bf16[2,128,256]{2,1,0:T(8,128)(2,1)S(1)}, u32[]{:S(2)}, u32[]{:S(2)}) %collective-permute-start.2) | collective-permute-done | bytes 131104 | tf_op jit(solution)/shard_map/ppermute | solution.py:15
  78.6 20.5 %collective-permute-start.3 = (bf16[2,128,128]{2,1,0:T(8,128)(2,1)S(1)}, bf16[2,128,128]{2,1,0:T(8,128)(2,1)S(1)}, u32[]{:S(2)}, u32[]{:S(2)}) collective-permute-start(bf16[2,128,128]{2,1,0:T(8,128)(2,1)S(1)} %fusion.128), channel_id=1, source_target_pairs={{0,16},{4,20},{8,24},{12,28},{1,17},{5,21},{9,25},{13,29},{2,18},{... | collective-permute-start | bytes 196616 | tf_op jit(solution)/shard_map/ppermute | solution.py:15
  99.3 2.9 collective-permute-done.3
  102.4 0.7 multiply_reduce_fusion.1
  104.1 2.3 collective-permute-done.4
  106.9 11.1 %collective-permute-done.5 = bf16[96,2048]{1,0:T(8,128)(2,1)S(1)} collective-permute-done((bf16[96,2048]{1,0:T(8,128)(2,1)S(1)}, bf16[96,2048]{1,0:T(8,128)(2,1)S(1)}, u32[]{:S(2)}, u32[]{:S(2)}) %collective-permute-start.5) | collective-permute-done | bytes 393248 | tf_op jit(solution)/shard_map/ppermute | solution.py:46
  118.8 10.0 %collective-permute-done.6 = bf16[96,2048]{1,0:T(8,128)(2,1)S(1)} collective-permute-done((bf16[96,2048]{1,0:T(8,128)(2,1)S(1)}, bf16[96,2048]{1,0:T(8,128)(2,1)S(1)}, u32[]{:S(2)}, u32[]{:S(2)}) %collective-permute-start.6) | collective-permute-done | bytes 393248 | tf_op jit(solution)/shard_map/ppermute | solution.py:46
  129.0 0.6 copy-done.7
  129.6 1.8 collective-permute-done.7
  131.4 7.1 %fusion.47 = f32[384,1408]{1,0:T(8,128)} fusion(bf16[2048,1408]{1,0:T(8,128)(2,1)} %all-gather.4.cloned.1.call-done, bf16[192,2048]{1,0:T(8,128)(2,1)} %collective-permute-done.7, bf16[96,2048]{1,0:T(8,128)(2,1)} %copy-done.7, bf16[96,2048]{1,0:T(8,128)(2,1)} %copy-done.2), kind=kOutput, calls=%fused_computation.75 | convolution fusion | flops 2219311104 | bytes 9502720 | tf_op jit(solution)/shard_map/dot_general | solution.py:297
  138.5 67.4 %all-gather.6.cloned.1.call-done = bf16[2048,1408]{1,0:T(8,128)(2,1)} async-done(((bf16[256,1408]{1,0:T(8,128)(2,1)}), bf16[2048,1408]{1,0:T(8,128)(2,1)}) %all-gather.6.cloned.1.call-update) | async-done | bytes 5767184 | tf_op jit(solution)/shard_map/all_gather | solution.py:263
  206.0 7.4 %multiply_convert_fusion = bf16[384,1408]{1,0:T(8,128)(2,1)} fusion(f32[384,1408]{1,0:T(8,128)} %fusion.47, bf16[2048,1408]{1,0:T(8,128)(2,1)} %all-gather.6.cloned.1.call-done, bf16[192,2048]{1,0:T(8,128)(2,1)} %collective-permute-done.7, bf16[96,2048]{1,0:T(8,128)(2,1)} %copy-done.7, bf16[96,2048]{1,0:T(8,128)(2,1)} %copy-done.2), kind=kOutput, calls=%fused_computation.46 | convolution fusion | flops 2222555136 | bytes 10584064 | tf_op jit(solution)/shard_map/dot_general | solution.py:298
  213.4 86.0 %all-gather.8.cloned.1.call-done = bf16[1408,2048]{1,0:T(8,128)(2,1)} async-done(((bf16[1408,256]{1,0:T(8,128)(2,1)}), bf16[1408,2048]{1,0:T(8,128)(2,1)}) %all-gather.8.cloned.1.call-update) | async-done | bytes 5767184 | tf_op jit(solution)/shard_map/all_gather | solution.py:264
  299.4 4.3 %convolution_convert_fusion = bf16[192,2048]{1,0:T(8,128)(2,1)S(1)} fusion(bf16[1408,2048]{1,0:T(8,128)(2,1)} %all-gather.8.cloned.1.call-done, bf16[384,1408]{1,0:T(8,128)(2,1)} %multiply_convert_fusion), kind=kOutput, calls=%fused_computation.44 | convolution fusion | flops 1107689472 | bytes 7094272 | tf_op jit(solution)/shard_map/dot_general | solution.py:71
  303.8 2.3 collective-permute-done.8
  306.1 1.4 convert_add_fusion
  307.5 1.6 collective-permute-start.9
  309.1 9.6 %collective-permute-done.9 = bf16[96,2048]{1,0:T(8,128)(2,1)S(1)} collective-permute-done((bf16[96,2048]{1,0:T(8,128)(2,1)S(1)}, bf16[96,2048]{1,0:T(8,128)(2,1)S(1)}, u32[]{:S(2)}, u32[]{:S(2)}) %collective-permute-start.9) | collective-permute-done | bytes 393248 | tf_op jit(solution)/shard_map/ppermute | solution.py:46
  318.7 1.0 fusion.40
  (135 shorter events, 13.4 us)
Async XLA Ops:
  6.5 97.1 %copy-start = (bf16[256,2048]{1,0:T(8,128)(2,1)S(1)}, bf16[256,2048]{1,0:T(8,128)(2,1)}, u32[]{:S(2)}) copy-start(bf16[256,2048]{1,0:T(8,128)(2,1)} %param.27) | copy-start | bytes 3145732
  6.5 2.3 copy-start.16
  6.5 2.4 copy-start.12
  6.5 2.4 copy-start.11
  6.5 2.5 copy-start.3
  6.5 3.0 copy-start.13
  6.6 124.9 %all-gather.4.cloned.1.call-start = ((), (), s32[]{:S(2)}) async-start(), calls=%async_computation | async-start | bytes 6488064 | tf_op jit(solution)/shard_map/all_gather | solution.py:262
  7.3 198.7 %all-gather.6.cloned.1.call-start = ((), (), s32[]{:S(2)}) async-start(), calls=%async_computation.1 | async-start | bytes 6488064 | tf_op jit(solution)/shard_map/all_gather | solution.py:263
  8.0 291.3 %all-gather.8.cloned.1.call-start = ((), (), s32[]{:S(2)}) async-start(), calls=%async_computation.2 | async-start | bytes 6488064 | tf_op jit(solution)/shard_map/all_gather | solution.py:264
  14.4 2.3 copy-start.4
  14.9 2.1 copy-start.8
  46.2 52.9 %copy-start.5 = (f32[6,2,64,128]{3,2,0,1:T(8,128)S(1)}, f32[6,2,64,128]{3,2,0,1:T(8,128)}, u32[]{:S(2)}) copy-start(f32[6,2,64,128]{3,2,0,1:T(8,128)} %get-tuple-element.70) | copy-start | bytes 1179652
  46.2 56.2 %copy-start.6 = (f32[6,2,64,128]{3,2,0,1:T(8,128)S(1)}, f32[6,2,64,128]{3,2,0,1:T(8,128)}, u32[]{:S(2)}) copy-start(f32[6,2,64,128]{3,2,0,1:T(8,128)} %get-tuple-element.71) | copy-start | bytes 1179652
  46.3 10.6 %collective-permute-start = (bf16[2,128,256]{2,1,0:T(8,128)(2,1)S(1)}, bf16[2,128,256]{2,1,0:T(8,128)(2,1)S(1)}, u32[]{:S(2)}, u32[]{:S(2)}) collective-permute-start(bf16[2,128,256]{2,1,0:T(8,128)(2,1)S(1)} %pad_maximum_fusion.6), channel_id=1, source_target_pairs={{0,4},{4,8},{8,12},{12,16},{16,20},{20,24},{24,28},{1,5},{5,9},{9,... | collective-permute-start | bytes 393224 | tf_op jit(solution)/shard_map/ppermute | solution.py:15
  56.9 9.8 %collective-permute-start.1 = (bf16[2,128,256]{2,1,0:T(8,128)(2,1)S(1)}, bf16[2,128,256]{2,1,0:T(8,128)(2,1)S(1)}, u32[]{:S(2)}, u32[]{:S(2)}) collective-permute-start(bf16[2,128,256]{2,1,0:T(8,128)(2,1)S(1)} %collective-permute-done), channel_id=1, source_target_pairs={{0,4},{4,8},{8,12},{12,16},{16,20},{20,24},{24,28},{1,5},{5,9},{9,... | collective-permute-start | bytes 393224 | tf_op jit(solution)/shard_map/ppermute | solution.py:15
  66.8 36.3 %copy-start.14 = (f32[128]{0:T(128)S(1)}, f32[128]{0:T(128)}, u32[]{:S(2)}) copy-start(f32[128]{0:T(128)} %param.26) | copy-start | bytes 1540
  66.9 11.4 %collective-permute-start.2 = (bf16[2,128,256]{2,1,0:T(8,128)(2,1)S(1)}, bf16[2,128,256]{2,1,0:T(8,128)(2,1)S(1)}, u32[]{:S(2)}, u32[]{:S(2)}) collective-permute-start(bf16[2,128,256]{2,1,0:T(8,128)(2,1)S(1)} %pad_maximum_fusion.7), channel_id=1, source_target_pairs={{0,8},{4,12},{8,16},{12,20},{16,24},{20,28},{1,9},{5,13},{9,17},{1... | collective-permute-start | bytes 393224 | tf_op jit(solution)/shard_map/ppermute | solution.py:15
  78.6 24.8 %copy-start.9 = (bf16[384,256]{1,0:T(8,128)(2,1)S(1)}, bf16[384,256]{1,0:T(8,128)(2,1)}, u32[]{:S(2)}) copy-start(bf16[384,256]{1,0:T(8,128)(2,1)} %param.21) | copy-start | bytes 589828
  78.6 23.6 %collective-permute-start.3 = (bf16[2,128,128]{2,1,0:T(8,128)(2,1)S(1)}, bf16[2,128,128]{2,1,0:T(8,128)(2,1)S(1)}, u32[]{:S(2)}, u32[]{:S(2)}) collective-permute-start(bf16[2,128,128]{2,1,0:T(8,128)(2,1)S(1)} %fusion.128), channel_id=1, source_target_pairs={{0,16},{4,20},{8,24},{12,28},{1,17},{5,21},{9,25},{13,29},{2,18},{... | collective-permute-start | bytes 196616 | tf_op jit(solution)/shard_map/ppermute | solution.py:15
  104.0 14.0 %copy-start.1 = (bf16[96,2048]{1,0:T(8,128)(2,1)S(1)}, bf16[96,2048]{1,0:T(8,128)(2,1)}, u32[]{:S(2)}) copy-start(bf16[96,2048]{1,0:T(8,128)(2,1)} %param.17) | copy-start | bytes 1179652
  104.0 2.4 collective-permute-start.4
  106.3 11.9 %copy-start.10 = (f32[2048]{0:T(1024)S(1)}, f32[2048]{0:T(1024)}, u32[]{:S(2)}) copy-start(f32[2048]{0:T(1024)} %param.28) | copy-start | bytes 24580
  106.8 11.2 %collective-permute-start.5 = (bf16[96,2048]{1,0:T(8,128)(2,1)S(1)}, bf16[96,2048]{1,0:T(8,128)(2,1)S(1)}, u32[]{:S(2)}, u32[]{:S(2)}) collective-permute-start(bf16[96,2048]{1,0:T(8,128)(2,1)S(1)} %slice.148), channel_id=1, source_target_pairs={{0,2},{1,3},{2,0},{3,1},{4,6},{5,7},{6,4},{7,5},{8,10},{9,11},{10,... | collective-permute-start | bytes 1179656 | tf_op jit(solution)/shard_map/ppermute | solution.py:46
  118.5 10.4 %copy-start.2 = (bf16[96,2048]{1,0:T(8,128)(2,1)}, bf16[96,2048]{1,0:T(8,128)(2,1)S(1)}, u32[]{:S(2)}) copy-start(bf16[96,2048]{1,0:T(8,128)(2,1)S(1)} %multiply_convert_fusion.1) | copy-start | bytes 1179652
  118.5 10.4 %collective-permute-start.6 = (bf16[96,2048]{1,0:T(8,128)(2,1)S(1)}, bf16[96,2048]{1,0:T(8,128)(2,1)S(1)}, u32[]{:S(2)}, u32[]{:S(2)}) collective-permute-start(bf16[96,2048]{1,0:T(8,128)(2,1)S(1)} %multiply_convert_fusion.1), channel_id=1, source_target_pairs={{0,2},{1,3},{2,0},{3,1},{4,6},{5,7},{6,4},{7,5},{8,10},{9,11},{10,... | collective-permute-start | bytes 1179656 | tf_op jit(solution)/shard_map/ppermute | solution.py:46
  128.9 0.7 copy-start.7
  128.9 2.5 collective-permute-start.7
  299.4 6.7 %copy-start.15 = (bf16[1408,2048]{1,0:T(8,128)(2,1)S(1)}, bf16[1408,2048]{1,0:T(8,128)(2,1)}, u32[]{:S(2)}) copy-start(bf16[1408,2048]{1,0:T(8,128)(2,1)} %all-gather.8.cloned.1.call-done) | copy-start | bytes 17301508
  299.4 6.7 %copy-start.17 = (bf16[384,1408]{1,0:T(8,128)(2,1)S(1)}, bf16[384,1408]{1,0:T(8,128)(2,1)}, u32[]{:S(2)}) copy-start(bf16[384,1408]{1,0:T(8,128)(2,1)} %multiply_convert_fusion) | copy-start | bytes 3244036
  303.7 2.4 collective-permute-start.8
  307.5 11.2 %collective-permute-start.9 = (bf16[96,2048]{1,0:T(8,128)(2,1)S(1)}, bf16[96,2048]{1,0:T(8,128)(2,1)S(1)}, u32[]{:S(2)}, u32[]{:S(2)}) collective-permute-start(bf16[96,2048]{1,0:T(8,128)(2,1)S(1)} %slice.147), channel_id=1, source_target_pairs={{0,2},{1,3},{2,0},{3,1},{4,6},{5,7},{6,4},{7,5},{8,10},{9,11},{10,... | collective-permute-start | bytes 1179656 | tf_op jit(solution)/shard_map/ppermute | solution.py:46
Sparse Core Ops, SparseCore 0:
  9.5 99.7 all-gather.3
  111.5 94.4 all-gather.5
  208.0 91.2 all-gather.7
where the time goes:
time: 327 us; the launch traced here: 326 us
  waiting for transfers between devices  212 us (65%)
  matrix products  55.6 us (17%)
  starting transfers between devices  38.3 us (12%)
  between operations  13.8 us (4%)
  other arithmetic  3.82 us (1%)
    all_gather x1, waiting for transfers between devices, body(): down_whole = lax.all_gather(down_matrix, 'sp', axis=1, tiled=True)  86 us
    all_gather x1, waiting for transfers between devices, body(): up_whole = lax.all_gather(up_matrix, 'sp', axis=0, tiled=True)  67.4 us
    ppermute x6, waiting for transfers between devices, swap(): return lax.ppermute(value, axis, [(i, i ^ bit) for i in range(size)])  37.2 us
    ppermute x4, starting transfers between devices, from_behind(): return lax.ppermute(value, axis, pairs)  35.9 us
    ppermute x4, waiting for transfers between devices, from_behind(): return lax.ppermute(value, axis, pairs)  19.2 us
    dot_general x1, matrix products, body(): up_total = jnp.dot(whole_rows, up_whole, preferred_element_type=jnp.float32)  7.38 us
    dot_general x1, matrix products, body(): jnp.dot(whole_rows, gate_whole, preferred_element_type=jnp.float32)  7.12 us
  transfers between devices with their start and end apart: 13, of which 12 were waited for; matrix products, arithmetic and copies ran while one was open for 17% of the time, Pallas kernels for 0%

commit v1 on v0

--- a/solution.py
+++ b/solution.py
@@ -260,7 +260,10 @@
     down_matrix,
 ):
     gate_whole = lax.all_gather(gate_matrix, "sp", axis=0, tiled=True)
-    up_whole = lax.all_gather(up_matrix, "sp", axis=0, tiled=True)
+    t1 = lax.all_to_all(
+        jnp.stack(lax.axis_size("sp") * [up_matrix], axis=0), "sp", split_axis=0, concat_axis=0
+    )
+    up_whole = jnp.concatenate(t1, 0)
     down_whole = lax.all_gather(down_matrix, "sp", axis=1, tiled=True)
     block_outputs, decay_spans, matrix_product, running_state, _ = local_recurrence(
         query_projected,

time: 327 us -> 337 us (1.031)
  starting transfers between devices: 38.3 us -> 190 us
  waiting for transfers between devices: 212 us -> 66.3 us
  local copies, waits for them, and re-layouts: 2.49 us -> 6.51 us
    ppermute x4, starting transfers between devices: 35.9 us -> 178 us  [from_behind(): return lax.ppermute(value, axis, pairs)]
    all_gather x1, waiting for transfers between devices: 86 us -> 10.8 us  [body(): down_whole = lax.all_gather(down_matrix, 'sp', axis=1, tiled=True)]
    all_gather x1 -> x0, waiting for transfers between devices: 67.4 us -> none  [body(): up_whole = lax.all_gather(up_matrix, 'sp', axis=0, tiled=True)]
    all_to_all x0 -> x1, starting transfers between devices: none -> 7.45 us  [body(): lax.all_to_all(jnp.stack(lax.axis_size('sp') * [up_matrix], axis=0), 'sp'...]
    another operation x0 -> x1, local copies, waits for them, and re-layouts: none -> 4 us  [body(): jnp.stack(lax.axis_size('sp') * [up_matrix], axis=0)]
  transfers between devices with their start and end apart: 13 -> 13, of which waited for: 12 -> 11; matrix products, arithmetic and copies ran while one was open for 17% -> 17% of each run, Pallas kernels for 0% -> 0%
where the time goes in v1:
time: 337 us
  starting transfers between devices  190 us (56%)
  waiting for transfers between devices  66.3 us (20%)
  matrix products  55.8 us (17%)
  between operations  14.1 us (4%)
  local copies, waits for them, and re-layouts  6.51 us (2%)
  other arithmetic  3.82 us (1%)
    ppermute x4, starting transfers between devices, from_behind(): return lax.ppermute(value, axis, pairs)  178 us
    ppermute x6, waiting for transfers between devices, swap(): return lax.ppermute(value, axis, [(i, i ^ bit) for i in range(size)])  34.8 us
    ppermute x4, waiting for transfers between devices, from_behind(): return lax.ppermute(value, axis, pairs)  19.4 us
    all_gather x1, waiting for transfers between devices, body(): down_whole = lax.all_gather(down_matrix, 'sp', axis=1, tiled=True)  10.8 us
    dot_general x1, matrix products, body(): up_total = jnp.dot(whole_rows, up_whole, preferred_element_type=jnp.float32)  7.53 us
    all_to_all x1, starting transfers between devices, body(): lax.all_to_all(jnp.stack(lax.axis_size('sp') * [up_matrix], axis=0), 'sp'...  7.45 us
    dot_general x1, matrix products, body(): jnp.dot(whole_rows, gate_whole, preferred_element_type=jnp.float32)  7.14 us
  transfers between devices with their start and end apart: 13, of which 11 were waited for; matrix products, arithmetic and copies ran while one was open for 17% of the time, Pallas kernels for 0%

profile of v1, /device:TPU:0, one launch (start us, length us, event | category | flops | bytes accessed | tf_op | source)
XLA Modules:
  0.0 336.7 jit_solution(8140016382743054053)
XLA Ops:
  6.5 0.7 all-gather.3.cloned.1.call-update
  7.3 4.0 %stack.2 = bf16[8,256,1408]{2,1,0:T(8,128)(2,1)} broadcast(bf16[256,1408]{1,0:T(8,128)(2,1)} %param.30), dimensions={1,2} | broadcast | bytes 6488064 | tf_op jit(solution)/shard_map/stack | solution.py:264
  11.3 7.5 %all-to-all-start = ((bf16[8,256,1408]{2,1,0:T(8,128)(2,1)}), bf16[8,256,1408]{2,1,0:T(8,128)(2,1)}, u32[]{:S(2)}, u32[]{:S(2)}) async-start(bf16[8,256,1408]{2,1,0:T(8,128)(2,1)} %stack.2), calls=%async_computation | async-start | bytes 11534336 | tf_op jit(solution)/shard_map/all_to_all | solution.py:263
  18.8 0.7 all-gather.5.cloned.1.call-update
  20.3 0.4 reduce_window_sum.11
  20.9 0.8 convolution_multiply_fusion
  21.9 0.5 fusion.73
  22.4 0.5 convolution_subtract_fusion.7
  23.0 0.5 fusion.71
  23.5 0.5 convolution_subtract_fusion.6
  24.0 0.5 fusion.69
  24.6 0.5 convolution_subtract_fusion.5
  25.1 0.5 fusion.67
  25.6 0.5 convolution_subtract_fusion.4
  26.2 0.5 fusion.65
  26.7 0.5 convolution_subtract_fusion.3
  28.2 0.8 fusion.42
  29.0 0.8 slice_bitcast_fusion
  29.8 0.8 fusion.38
  30.7 26.2 %while.17 = (s32[]{:T(128)}, f32[2,128,128]{2,1,0:T(8,128)S(1)}, f32[2,128,128]{2,1,0:T(8,128)S(1)}, f32[6,2,64,128]{3,2,0,1:T(8,128)}, f32[6,2,64,128]{3,2,0,1:...) while((s32[]{:T(128)}, f32[2,128,128]{2,1,0:T(8,128)S(1)}, ...), condition=%wide.region_4.5_spmd.clone, body=%wide.region_3.4_spmd.clone.sunk | while | flops 201605120 | bytes 2758829 | solution.py:229
  30.7 1.1 convolution_subtract_fusion.11
  32.1 0.8 fusion.205
  33.5 0.9 fusion.206
  35.1 1.1 convolution_subtract_fusion.11
  36.4 0.8 fusion.205
  37.9 0.9 fusion.206
  39.5 1.1 convolution_subtract_fusion.11
  40.8 0.8 fusion.205
  41.7 0.4 convolution_add_fusion.5
  42.3 0.9 fusion.206
  43.9 1.1 convolution_subtract_fusion.11
  45.2 0.8 fusion.205
  46.7 0.9 fusion.206
  48.2 1.1 convolution_subtract_fusion.11
  49.6 0.8 fusion.205
  51.0 0.9 fusion.206
  52.6 1.1 convolution_subtract_fusion.11
  54.0 0.8 fusion.205
  55.4 0.9 fusion.206
  57.1 4.1 %collective-permute-start = (bf16[2,128,256]{2,1,0:T(8,128)(2,1)S(1)}, bf16[2,128,256]{2,1,0:T(8,128)(2,1)S(1)}, u32[]{:S(2)}, u32[]{:S(2)}) collective-permute-start(bf16[2,128,256]{2,1,0:T(8,128)(2,1)S(1)} %pad_maximum_fusion.6), channel_id=1, source_target_pairs={{0,4},{4,8},{8,12},{12,16},{16,20},{20,24},{24,28},{1,5},{5,9},{9,... | collective-permute-start | bytes 393224 | tf_op jit(solution)/shard_map/ppermute | solution.py:15
  61.1 9.6 %collective-permute-done = bf16[2,128,256]{2,1,0:T(8,128)(2,1)S(1)} collective-permute-done((bf16[2,128,256]{2,1,0:T(8,128)(2,1)S(1)}, bf16[2,128,256]{2,1,0:T(8,128)(2,1)S(1)}, u32[]{:S(2)}, u32[]{:S(2)}) %collective-permute-start) | collective-permute-done | bytes 131104 | tf_op jit(solution)/shard_map/ppermute | solution.py:15
  70.7 92.2 %collective-permute-start.1 = (bf16[2,128,256]{2,1,0:T(8,128)(2,1)S(1)}, bf16[2,128,256]{2,1,0:T(8,128)(2,1)S(1)}, u32[]{:S(2)}, u32[]{:S(2)}) collective-permute-start(bf16[2,128,256]{2,1,0:T(8,128)(2,1)S(1)} %collective-permute-done), channel_id=1, source_target_pairs={{0,4},{4,8},{8,12},{12,16},{16,20},{20,24},{24,28},{1,5},{5,9},{9,... | collective-permute-start | bytes 393224 | tf_op jit(solution)/shard_map/ppermute | solution.py:15
  162.8 3.1 collective-permute-done.1
  166.2 62.4 %collective-permute-start.2 = (bf16[2,128,256]{2,1,0:T(8,128)(2,1)S(1)}, bf16[2,128,256]{2,1,0:T(8,128)(2,1)S(1)}, u32[]{:S(2)}, u32[]{:S(2)}) collective-permute-start(bf16[2,128,256]{2,1,0:T(8,128)(2,1)S(1)} %pad_maximum_fusion.7), channel_id=1, source_target_pairs={{0,8},{4,12},{8,16},{12,20},{16,24},{20,28},{1,9},{5,13},{9,17},{1... | collective-permute-start | bytes 393224 | tf_op jit(solution)/shard_map/ppermute | solution.py:15
  228.6 5.0 %collective-permute-done.2 = bf16[2,128,256]{2,1,0:T(8,128)(2,1)S(1)} collective-permute-done((bf16[2,128,256]{2,1,0:T(8,128)(2,1)S(1)}, bf16[2,128,256]{2,1,0:T(8,128)(2,1)S(1)}, u32[]{:S(2)}, u32[]{:S(2)}) %collective-permute-start.2) | collective-permute-done | bytes 131104 | tf_op jit(solution)/shard_map/ppermute | solution.py:15
  233.9 19.0 %collective-permute-start.3 = (bf16[2,128,128]{2,1,0:T(8,128)(2,1)S(1)}, bf16[2,128,128]{2,1,0:T(8,128)(2,1)S(1)}, u32[]{:S(2)}, u32[]{:S(2)}) collective-permute-start(bf16[2,128,128]{2,1,0:T(8,128)(2,1)S(1)} %fusion.128), channel_id=1, source_target_pairs={{0,16},{4,20},{8,24},{12,28},{1,17},{5,21},{9,25},{13,29},{2,18},{... | collective-permute-start | bytes 196616 | tf_op jit(solution)/shard_map/ppermute | solution.py:15
  253.1 1.7 collective-permute-done.3
  255.0 0.7 multiply_reduce_fusion.1
  256.6 2.3 collective-permute-done.4
  259.3 1.4 collective-permute-start.5
  260.8 9.8 %collective-permute-done.5 = bf16[96,2048]{1,0:T(8,128)(2,1)S(1)} collective-permute-done((bf16[96,2048]{1,0:T(8,128)(2,1)S(1)}, bf16[96,2048]{1,0:T(8,128)(2,1)S(1)}, u32[]{:S(2)}, u32[]{:S(2)}) %collective-permute-start.5) | collective-permute-done | bytes 393248 | tf_op jit(solution)/shard_map/ppermute | solution.py:46
  271.0 1.4 collective-permute-start.6
  272.5 9.0 %collective-permute-done.6 = bf16[96,2048]{1,0:T(8,128)(2,1)S(1)} collective-permute-done((bf16[96,2048]{1,0:T(8,128)(2,1)S(1)}, bf16[96,2048]{1,0:T(8,128)(2,1)S(1)}, u32[]{:S(2)}, u32[]{:S(2)}) %collective-permute-start.6) | collective-permute-done | bytes 393248 | tf_op jit(solution)/shard_map/ppermute | solution.py:46
  281.6 0.6 copy-done.7
  282.2 1.8 collective-permute-done.7
  284.1 7.1 %fusion.47 = f32[384,1408]{1,0:T(8,128)} fusion(bf16[2048,1408]{1,0:T(8,128)(2,1)} %all-gather.3.cloned.1.call-done, bf16[192,2048]{1,0:T(8,128)(2,1)} %collective-permute-done.7, bf16[96,2048]{1,0:T(8,128)(2,1)} %copy-done.7, bf16[96,2048]{1,0:T(8,128)(2,1)} %copy-done.2), kind=kOutput, calls=%fused_computation.75 | convolution fusion | flops 2219311104 | bytes 9502720 | tf_op jit(solution)/shard_map/dot_general | solution.py:300
  291.2 7.5 %multiply_convert_fusion = bf16[384,1408]{1,0:T(8,128)(2,1)} fusion(f32[384,1408]{1,0:T(8,128)} %fusion.47, bf16[2048,1408]{1,0:T(8,128)(2,1)} %bitcast.24, bf16[192,2048]{1,0:T(8,128)(2,1)} %collective-permute-done.7, bf16[96,2048]{1,0:T(8,128)(2,1)} %copy-done.7, bf16[96,2048]{1,0:T(8,128)(2,1)} %copy-done.2), kind=kOutput, calls=%fused_computation.46 | convolution fusion | flops 2222555136 | bytes 10584064 | tf_op jit(solution)/shard_map/dot_general | solution.py:301
  298.7 10.8 %all-gather.5.cloned.1.call-done = bf16[1408,2048]{1,0:T(8,128)(2,1)} async-done(((bf16[1408,256]{1,0:T(8,128)(2,1)}), bf16[1408,2048]{1,0:T(8,128)(2,1)}) %all-gather.5.cloned.1.call-update) | async-done | bytes 5767184 | tf_op jit(solution)/shard_map/all_gather | solution.py:267
  309.5 4.3 %convolution_convert_fusion = bf16[192,2048]{1,0:T(8,128)(2,1)S(1)} fusion(bf16[1408,2048]{1,0:T(8,128)(2,1)} %all-gather.5.cloned.1.call-done, bf16[384,1408]{1,0:T(8,128)(2,1)} %multiply_convert_fusion), kind=kOutput, calls=%fused_computation.44 | convolution fusion | flops 1107689472 | bytes 7094272 | tf_op jit(solution)/shard_map/dot_general | solution.py:71
  313.9 2.3 collective-permute-done.8
  316.2 1.4 convert_add_fusion
  317.6 1.6 collective-permute-start.9
  319.2 9.6 %collective-permute-done.9 = bf16[96,2048]{1,0:T(8,128)(2,1)S(1)} collective-permute-done((bf16[96,2048]{1,0:T(8,128)(2,1)S(1)}, bf16[96,2048]{1,0:T(8,128)(2,1)S(1)}, u32[]{:S(2)}, u32[]{:S(2)}) %collective-permute-start.9) | collective-permute-done | bytes 393248 | tf_op jit(solution)/shard_map/ppermute | solution.py:46
  328.9 1.0 fusion.40
  (135 shorter events, 13.7 us)
Async XLA Ops:
  6.5 249.6 %copy-start = (bf16[256,2048]{1,0:T(8,128)(2,1)S(1)}, bf16[256,2048]{1,0:T(8,128)(2,1)}, u32[]{:S(2)}) copy-start(bf16[256,2048]{1,0:T(8,128)(2,1)} %param.27) | copy-start | bytes 3145732
  6.5 277.5 %all-gather.3.cloned.1.call-start = ((), (), s32[]{:S(2)}) async-start(), calls=%async_computation.1 | async-start | bytes 6488064 | tf_op jit(solution)/shard_map/all_gather | solution.py:262
  11.3 8.3 %copy-start.16 = (f32[2]{0:T(128)S(1)}, f32[2]{0:T(128)}, u32[]{:S(2)}) copy-start(f32[2]{0:T(128)} %param.25) | copy-start | bytes 28
  11.3 8.3 %copy-start.11 = (f32[2,384]{1,0:T(2,128)S(1)}, f32[2,384]{1,0:T(2,128)}, u32[]{:S(2)}) copy-start(f32[2,384]{1,0:T(2,128)} %param.24) | copy-start | bytes 9220
  11.3 8.4 %copy-start.12 = (bf16[2,384]{1,0:T(2,128)(2,1)S(1)}, bf16[2,384]{1,0:T(2,128)(2,1)}, u32[]{:S(2)}) copy-start(bf16[2,384]{1,0:T(2,128)(2,1)} %param.23) | copy-start | bytes 4612
  11.3 8.5 %copy-start.3 = (bf16[384,256]{1,0:T(8,128)(2,1)S(1)}, bf16[384,256]{1,0:T(8,128)(2,1)}, u32[]{:S(2)}) copy-start(bf16[384,256]{1,0:T(8,128)(2,1)} %param.19) | copy-start | bytes 589828
  11.3 9.0 %copy-start.13 = (bf16[2,384]{1,0:T(2,128)(2,1)S(1)}, bf16[2,384]{1,0:T(2,128)(2,1)}, u32[]{:S(2)}) copy-start(bf16[2,384]{1,0:T(2,128)(2,1)} %param.22) | copy-start | bytes 4612
  11.3 279.9 %all-to-all-start = ((bf16[8,256,1408]{2,1,0:T(8,128)(2,1)}), bf16[8,256,1408]{2,1,0:T(8,128)(2,1)}, u32[]{:S(2)}, u32[]{:S(2)}) async-start(bf16[8,256,1408]{2,1,0:T(8,128)(2,1)} %stack.2), calls=%async_computation | async-start | bytes 11534336 | tf_op jit(solution)/shard_map/all_to_all | solution.py:263
  18.7 290.8 %all-gather.5.cloned.1.call-start = ((), (), s32[]{:S(2)}) async-start(), calls=%async_computation.2 | async-start | bytes 6488064 | tf_op jit(solution)/shard_map/all_gather | solution.py:267
  25.1 2.2 copy-start.4
  25.6 2.1 copy-start.8
  57.0 195.9 %copy-start.5 = (f32[6,2,64,128]{3,2,0,1:T(8,128)S(1)}, f32[6,2,64,128]{3,2,0,1:T(8,128)}, u32[]{:S(2)}) copy-start(f32[6,2,64,128]{3,2,0,1:T(8,128)} %get-tuple-element.70) | copy-start | bytes 1179652
  57.0 198.0 %copy-start.6 = (f32[6,2,64,128]{3,2,0,1:T(8,128)S(1)}, f32[6,2,64,128]{3,2,0,1:T(8,128)}, u32[]{:S(2)}) copy-start(f32[6,2,64,128]{3,2,0,1:T(8,128)} %get-tuple-element.71) | copy-start | bytes 1179652
  57.1 13.6 %collective-permute-start = (bf16[2,128,256]{2,1,0:T(8,128)(2,1)S(1)}, bf16[2,128,256]{2,1,0:T(8,128)(2,1)S(1)}, u32[]{:S(2)}, u32[]{:S(2)}) collective-permute-start(bf16[2,128,256]{2,1,0:T(8,128)(2,1)S(1)} %pad_maximum_fusion.6), channel_id=1, source_target_pairs={{0,4},{4,8},{8,12},{12,16},{16,20},{20,24},{24,28},{1,5},{5,9},{9,... | collective-permute-start | bytes 393224 | tf_op jit(solution)/shard_map/ppermute | solution.py:15
  70.7 95.3 %collective-permute-start.1 = (bf16[2,128,256]{2,1,0:T(8,128)(2,1)S(1)}, bf16[2,128,256]{2,1,0:T(8,128)(2,1)S(1)}, u32[]{:S(2)}, u32[]{:S(2)}) collective-permute-start(bf16[2,128,256]{2,1,0:T(8,128)(2,1)S(1)} %collective-permute-done), channel_id=1, source_target_pairs={{0,4},{4,8},{8,12},{12,16},{16,20},{20,24},{24,28},{1,5},{5,9},{9,... | collective-permute-start | bytes 393224 | tf_op jit(solution)/shard_map/ppermute | solution.py:15
  166.1 89.5 %copy-start.14 = (f32[128]{0:T(128)S(1)}, f32[128]{0:T(128)}, u32[]{:S(2)}) copy-start(f32[128]{0:T(128)} %param.26) | copy-start | bytes 1540
  166.2 67.4 %collective-permute-start.2 = (bf16[2,128,256]{2,1,0:T(8,128)(2,1)S(1)}, bf16[2,128,256]{2,1,0:T(8,128)(2,1)S(1)}, u32[]{:S(2)}, u32[]{:S(2)}) collective-permute-start(bf16[2,128,256]{2,1,0:T(8,128)(2,1)S(1)} %pad_maximum_fusion.7), channel_id=1, source_target_pairs={{0,8},{4,12},{8,16},{12,20},{16,24},{20,28},{1,9},{5,13},{9,17},{1... | collective-permute-start | bytes 393224 | tf_op jit(solution)/shard_map/ppermute | solution.py:15
  233.9 22.1 %copy-start.9 = (bf16[384,256]{1,0:T(8,128)(2,1)S(1)}, bf16[384,256]{1,0:T(8,128)(2,1)}, u32[]{:S(2)}) copy-start(bf16[384,256]{1,0:T(8,128)(2,1)} %param.21) | copy-start | bytes 589828
  233.9 20.9 %collective-permute-start.3 = (bf16[2,128,128]{2,1,0:T(8,128)(2,1)S(1)}, bf16[2,128,128]{2,1,0:T(8,128)(2,1)S(1)}, u32[]{:S(2)}, u32[]{:S(2)}) collective-permute-start(bf16[2,128,128]{2,1,0:T(8,128)(2,1)S(1)} %fusion.128), channel_id=1, source_target_pairs={{0,16},{4,20},{8,24},{12,28},{1,17},{5,21},{9,25},{13,29},{2,18},{... | collective-permute-start | bytes 196616 | tf_op jit(solution)/shard_map/ppermute | solution.py:15
  256.5 14.0 %copy-start.1 = (bf16[96,2048]{1,0:T(8,128)(2,1)S(1)}, bf16[96,2048]{1,0:T(8,128)(2,1)}, u32[]{:S(2)}) copy-start(bf16[96,2048]{1,0:T(8,128)(2,1)} %param.17) | copy-start | bytes 1179652
  256.5 2.4 collective-permute-start.4
  258.9 11.9 %copy-start.10 = (f32[2048]{0:T(1024)S(1)}, f32[2048]{0:T(1024)}, u32[]{:S(2)}) copy-start(f32[2048]{0:T(1024)} %param.28) | copy-start | bytes 24580
  259.3 11.2 %collective-permute-start.5 = (bf16[96,2048]{1,0:T(8,128)(2,1)S(1)}, bf16[96,2048]{1,0:T(8,128)(2,1)S(1)}, u32[]{:S(2)}, u32[]{:S(2)}) collective-permute-start(bf16[96,2048]{1,0:T(8,128)(2,1)S(1)} %slice.148), channel_id=1, source_target_pairs={{0,2},{1,3},{2,0},{3,1},{4,6},{5,7},{6,4},{7,5},{8,10},{9,11},{10,... | collective-permute-start | bytes 1179656 | tf_op jit(solution)/shard_map/ppermute | solution.py:46
  271.0 10.5 %copy-start.2 = (bf16[96,2048]{1,0:T(8,128)(2,1)}, bf16[96,2048]{1,0:T(8,128)(2,1)S(1)}, u32[]{:S(2)}) copy-start(bf16[96,2048]{1,0:T(8,128)(2,1)S(1)} %multiply_convert_fusion.1) | copy-start | bytes 1179652
  271.0 10.5 %collective-permute-start.6 = (bf16[96,2048]{1,0:T(8,128)(2,1)S(1)}, bf16[96,2048]{1,0:T(8,128)(2,1)S(1)}, u32[]{:S(2)}, u32[]{:S(2)}) collective-permute-start(bf16[96,2048]{1,0:T(8,128)(2,1)S(1)} %multiply_convert_fusion.1), channel_id=1, source_target_pairs={{0,2},{1,3},{2,0},{3,1},{4,6},{5,7},{6,4},{7,5},{8,10},{9,11},{10,... | collective-permute-start | bytes 1179656 | tf_op jit(solution)/shard_map/ppermute | solution.py:46
  281.5 0.7 copy-start.7
  281.6 2.5 collective-permute-start.7
  309.5 6.7 %copy-start.15 = (bf16[1408,2048]{1,0:T(8,128)(2,1)S(1)}, bf16[1408,2048]{1,0:T(8,128)(2,1)}, u32[]{:S(2)}) copy-start(bf16[1408,2048]{1,0:T(8,128)(2,1)} %all-gather.5.cloned.1.call-done) | copy-start | bytes 17301508
  309.5 6.7 %copy-start.17 = (bf16[384,1408]{1,0:T(8,128)(2,1)S(1)}, bf16[384,1408]{1,0:T(8,128)(2,1)}, u32[]{:S(2)}) copy-start(bf16[384,1408]{1,0:T(8,128)(2,1)} %multiply_convert_fusion) | copy-start | bytes 3244036
  313.8 2.4 collective-permute-start.8
  317.6 11.2 %collective-permute-start.9 = (bf16[96,2048]{1,0:T(8,128)(2,1)S(1)}, bf16[96,2048]{1,0:T(8,128)(2,1)S(1)}, u32[]{:S(2)}, u32[]{:S(2)}) collective-permute-start(bf16[96,2048]{1,0:T(8,128)(2,1)S(1)} %slice.147), channel_id=1, source_target_pairs={{0,2},{1,3},{2,0},{3,1},{4,6},{5,7},{6,4},{7,5},{8,10},{9,11},{10,... | collective-permute-start | bytes 1179656 | tf_op jit(solution)/shard_map/ppermute | solution.py:46
Sparse Core Ops, SparseCore 0:
  9.5 199.5 all-gather.2
  211.1 98.3 all-gather.4
